TPU v7x, 32 devices: a whole 2x2x4 slice. The times are simulated.
32 devices in a mesh: sp: 8 (over z, x), tp: 4 (over y, core).
Axes of the slice: x: 2, y: 2, z: 4, core: 2. Of those that a mesh axis runs over, the one named last changes fastest.
Arguments:
- residual_in: bfloat16 [2048, 2048], P(('sp', 'tp')), may hold values from -0.119628906 to 0.119628906
- queries: bfloat16 [2048, 2048], P('sp', 'tp'), may hold values from -6 to 6
- keys_raw: bfloat16 [2048, 512], P('sp', 'tp'), may hold values from -6 to 6
- values_raw: bfloat16 [2048, 512], P('sp', 'tp'), may hold values from -6 to 6
- query_gain: float32 [128], replicated, may hold values from 0.28 to 7
- key_gain: float32 [128], replicated, may hold values from 0.28 to 7
- out_weight: bfloat16 [2048, 2048], P('tp'), may hold values from -0.125 to 0.125
- norm_gain: float32 [2048], replicated, may hold values from 0.1 to 1.9
- gate_weight: bfloat16 [2048, 5632], P('sp', 'tp'), may hold values from -0.125 to 0.125
- up_weight: bfloat16 [2048, 5632], P('sp', 'tp'), may hold values from -0.125 to 0.125
- down_weight: bfloat16 [5632, 2048], P('tp', 'sp'), may hold values from -0.078125 to 0.078125
Outputs:
- residual_out: bfloat16 [2048, 2048], P(('sp', 'tp'))
All inputs are finite; a program needn't handle non-finite values.
Results may differ from a plain program's by a relative error of at most 0.024.
The roundings to bfloat16 on the way count: a program that leaves them out, or rounds other values in their place, can miss the bound.
Values may be sent and summed in bfloat16 or wider, within the bound.
A program may use at most 128 MiB of HBM per device.

v0:
```python
import jax
import jax.numpy as jnp
from jax import lax
from jax.sharding import PartitionSpec as P

GRID_W = 64
EPS = 1e-06
THETA = 10000.0


def turn_half(part, angles):
    quarter = part.shape[-1] // 2
    cosine = jnp.cos(angles)[:, None, :]
    sine = jnp.sin(angles)[:, None, :]
    first = part[..., :quarter]
    second = part[..., quarter:]
    return part * cosine + jnp.concatenate([-second, first], axis=-1) * sine


def prepare_heads(raw, gain, positions, heads):
    count = raw.shape[0]
    head_dim = gain.shape[0]
    half = head_dim // 2
    vec = raw.astype(jnp.float32).reshape(count, heads, head_dim)
    vec = vec * lax.rsqrt(jnp.mean(vec * vec, axis=-1, keepdims=True) + EPS) * gain
    freqs = THETA ** (-jnp.arange(0, half, 2, dtype=jnp.float32) / half)
    row_ang = (positions // GRID_W).astype(jnp.float32)[:, None] * freqs
    col_ang = (positions % GRID_W).astype(jnp.float32)[:, None] * freqs
    row_ang = jnp.concatenate([row_ang, row_ang], axis=-1)
    col_ang = jnp.concatenate([col_ang, col_ang], axis=-1)
    turned = jnp.concatenate(
        [turn_half(vec[..., :half], row_ang), turn_half(vec[..., half:], col_ang)], axis=-1
    )
    return turned.astype(jnp.bfloat16)


def per_device(
    residual_in,
    queries,
    keys_raw,
    values_raw,
    query_gain,
    key_gain,
    out_weight,
    norm_gain,
    gate_weight,
    up_weight,
    down_weight,
):
    tok = queries.shape[0]
    head_dim = query_gain.shape[0]
    local_heads = queries.shape[1] // head_dim
    local_kv = keys_raw.shape[1] // head_dim
    group = local_heads // local_kv
    gate_full, up_full = (
        lax.all_gather(gate_weight, "sp", axis=0, tiled=True),
        lax.all_gather(up_weight, "sp", axis=0, tiled=True),
    )
    down_full = lax.all_gather(down_weight, "sp", axis=1, tiled=True)
    positions = lax.axis_index("sp") * tok + jnp.arange(tok, dtype=jnp.int32)
    q_rot = prepare_heads(queries, query_gain, positions, local_heads).reshape(
        tok, local_kv, group, head_dim
    )
    k_rot = prepare_heads(keys_raw, key_gain, positions, local_kv)
    vals = values_raw.reshape(tok, local_kv, head_dim)
    start_state = (
        jnp.full((tok, local_kv, group), -jnp.inf, jnp.float32),
        jnp.zeros((tok, local_kv, group), jnp.float32),
        jnp.zeros((tok, local_kv, group, head_dim), jnp.float32),
    )
    carry = start_state
    k_piece = lax.all_gather(k_rot, "sp", axis=0, tiled=True)
    v_piece = lax.all_gather(vals, "sp", axis=0, tiled=True)
    length = k_piece.shape[0]
    shards = length // tok
    per_step = max(1, 2048 // tok)
    factor = max((d for d in range(1, shards + 1) if shards % d == 0 and d <= per_step))
    span = factor * tok
    k_blocks = k_piece.reshape(length // span, span, local_kv, head_dim)
    v_blocks = v_piece.reshape(length // span, span, local_kv, head_dim)

    def step(state, blocks):
        top, total, summed = state
        k_blk, v_blk = blocks
        scores = jnp.einsum(
            "qkgd,skd->qkgs", q_rot, k_blk, preferred_element_type=jnp.float32
        ) * head_dim ** (-0.5)
        new_top = jnp.maximum(top, jnp.max(scores, axis=-1))
        shrink = jnp.exp(top - new_top)
        expo = jnp.exp(scores - new_top[..., None])
        total = total * shrink + jnp.sum(expo, axis=-1)
        summed = summed * shrink[..., None] + jnp.einsum(
            "qkgs,skd->qkgd", expo.astype(jnp.bfloat16), v_blk, preferred_element_type=jnp.float32
        )
        return ((new_top, total, summed), None)

    carry, _ = lax.scan(step, carry, (k_blocks, v_blocks))
    top, total, summed = carry
    attended = (summed / total[..., None]).astype(jnp.bfloat16).reshape(tok, local_heads * head_dim)
    projected = lax.psum_scatter(
        jnp.dot(attended, out_weight, preferred_element_type=jnp.float32).astype(jnp.bfloat16),
        "tp",
        scatter_dimension=0,
        tiled=True,
    ).astype(jnp.float32)
    mixed = (residual_in.astype(jnp.float32) + projected).astype(jnp.bfloat16)
    mixed_f = mixed.astype(jnp.float32)
    normed = (
        mixed_f * lax.rsqrt(jnp.mean(mixed_f * mixed_f, axis=-1, keepdims=True) + EPS) * norm_gain
    ).astype(jnp.bfloat16)
    whole_rows = lax.all_gather(normed, "tp", axis=0, tiled=True)
    gate = jnp.dot(whole_rows, gate_full, preferred_element_type=jnp.float32)
    up_val = jnp.dot(whole_rows, up_full, preferred_element_type=jnp.float32)
    hidden = (jax.nn.silu(gate) * up_val).astype(jnp.bfloat16)
    terms = jnp.dot(hidden, down_full, preferred_element_type=jnp.float32)
    fed = lax.psum_scatter(
        terms.astype(jnp.bfloat16), "tp", scatter_dimension=0, tiled=True
    ).astype(jnp.float32)
    return (mixed_f + 0.5 * fed).astype(jnp.bfloat16)


def solution(mesh):
    placed = (
        P(("sp", "tp"), None),
        P("sp", "tp"),
        P("sp", "tp"),
        P("sp", "tp"),
        P(),
        P(),
        P("tp", None),
        P(),
        P("sp", "tp"),
        P("sp", "tp"),
        P("tp", "sp"),
    )
    return jax.shard_map(
        per_device, mesh=mesh, in_specs=placed, out_specs=P(("sp", "tp"), None), check_vma=False
    )
```

profile of v0, /device:TPU:0, one launch (start us, length us, event | category | flops | bytes accessed | tf_op | source)
XLA Modules:
  0.0 460.9 jit_solution(13443270139341550448)
XLA Ops:
  6.5 0.0 copy-start
  6.5 0.0 reduce-scatter.3.cloned.1.call-start
  6.6 1.1 fusion.33
  7.7 0.9 fusion.35
  8.6 0.2 slice_negate_fusion.3
  8.8 0.8 broadcast_multiply_fusion.1
  9.6 1.2 fusion.39
  10.8 0.1 pad_maximum_fusion.4
  10.9 33.0 %all_gather.18 = bf16[2048,1,128]{2,0,1:T(8,128)(2,1)S(1)} all-gather(bf16[256,1,128]{2,0,1:T(8,128)(2,1)S(1)} %pad_maximum_fusion.4), channel_id=1, replica_groups=mesh['sp'=8,'tp'=4] {'sp'}, dimensions={0}, use_global_device_ids=true | all-gather | bytes 589824 | tf_op jit(solution)/shard_map/all_gather | solution.py:72
  43.9 1.1 copy.14
  45.0 0.1 multiply_reduce_fusion
  45.1 0.1 copy.15
  45.2 0.9 multiply_multiply_fusion
  46.1 0.5 slice_negate_fusion.1
  46.6 1.5 fusion.43
  48.1 0.5 fusion.41
  48.7 0.5 fusion.26
  49.1 1.3 bitcast_reduce_fusion
  50.5 0.0 copy-start.1
  50.5 0.0 copy-start.4
  50.5 3.2 copy-done.1
  53.7 1.4 fusion.1
  55.1 0.0 copy-done.4
  55.1 0.1 copy.16
  55.2 31.3 %all-gather = bf16[2048,128]{0,1:T(8,128)(2,1)S(1)} all-gather(bf16[256,128]{0,1:T(8,128)(2,1)S(1)} %copy.16), channel_id=2, replica_groups=mesh['sp'=8,'tp'=4] {'sp'}, dimensions={0}, use_global_device_ids=true | all-gather | bytes 589824 | tf_op jit(solution)/shard_map/all_gather | solution.py:73
  86.5 0.0 copy-start.2
  86.5 0.0 copy-start.5
  86.5 5.1 %fusion.16 = bf16[1,128,256,4]{2,1,3,0:T(8,128)(2,1)S(1)} fusion(f32[2048,256,4]{1,0,2:T(8,128)} %copy-done.1, f32[256,4]{0,1:T(4,128)S(1)} %get-tuple-element.50, bf16[2048,128]{0,1:T(8,128)(2,1)S(1)} %all-gather, f32[256,4]{0,1:T(4,128)S(1)} %get-tuple-element.43, f32[256,4]{0,1:T(4,128)S(1)} %get-tuple-element.42), kind=kOutput, calls=%fused_computation.14 | convolution fusion | flops 543555584 | bytes 9187328 | tf_op jit(solution)/shard_map/while/body/eval_jaxpr/qkgs,skd->qkgd/dot_general | solution.py:92
  91.6 0.0 copy-done
  91.6 1.7 convolution_convert_fusion
  93.3 0.0 reduce-scatter.3.cloned.1.call-update
  93.3 0.0 all-gather.6.cloned.1.call-start
  93.4 26.1 %reduce-scatter.3.cloned.1.call-done = bf16[64,2048]{1,0:T(8,128)(2,1)} async-done(((bf16[256,2048]{1,0:T(8,128)(2,1)}), bf16[64,2048]{1,0:T(8,128)(2,1)}) %reduce-scatter.3.cloned.1.call-update) | async-done | bytes 262160 | tf_op jit(solution)/shard_map/reduce_scatter | solution.py:100
  119.4 0.0 copy-done.2
  119.4 1.1 fusion.19
  120.6 0.0 copy-done.5
  120.6 1.8 fusion.21
  122.4 0.0 all-gather.6.cloned.1.call-update
  122.4 0.0 all-gather.8.cloned.1.call-start
  122.5 0.7 all-gather.8.cloned.1.call-update
  123.1 0.0 all-gather.10.cloned.1.call-start
  123.2 0.5 all-gather.10.cloned.1.call-update
  123.7 0.0 all-gather.12.cloned.1.call-start
  123.8 0.5 all-gather.12.cloned.1.call-update
  124.3 0.2 reduce-scatter.5.cloned.1.call-start
  124.5 14.7 %all-gather.6.cloned.1.call-done = bf16[256,2048]{1,0:T(8,128)(2,1)} async-done(((bf16[64,2048]{1,0:T(8,128)(2,1)}), bf16[256,2048]{1,0:T(8,128)(2,1)}) %all-gather.6.cloned.1.call-update) | async-done | bytes 1048592 | tf_op jit(solution)/shard_map/all_gather | solution.py:111
  139.3 94.5 %all-gather.8.cloned.1.call-done = bf16[2048,1408]{1,0:T(8,128)(2,1)} async-done(((bf16[256,1408]{1,0:T(8,128)(2,1)}), bf16[2048,1408]{1,0:T(8,128)(2,1)}) %all-gather.8.cloned.1.call-update) | async-done | bytes 5767184 | tf_op jit(solution)/shard_map/all_gather | solution.py:56
  233.8 5.9 %fusion.53 = f32[256,1408]{1,0:T(8,128)} fusion(bf16[256,2048]{1,0:T(8,128)(2,1)} %all-gather.6.cloned.1.call-done, bf16[2048,1408]{1,0:T(8,128)(2,1)} %all-gather.8.cloned.1.call-done), kind=kOutput, calls=%fused_computation.88 | convolution fusion | flops 1476395008 | bytes 8257536 | tf_op jit(solution)/shard_map/dot_general | solution.py:112
  239.7 0.0 copy-start.3
  239.7 86.7 %all-gather.10.cloned.1.call-done = bf16[2048,1408]{1,0:T(8,128)(2,1)} async-done(((bf16[256,1408]{1,0:T(8,128)(2,1)}), bf16[2048,1408]{1,0:T(8,128)(2,1)}) %all-gather.10.cloned.1.call-update) | async-done | bytes 5767184 | tf_op jit(solution)/shard_map/all_gather | solution.py:57
  326.3 93.2 %all-gather.12.cloned.1.call-done = bf16[1408,2048]{1,0:T(8,128)(2,1)} async-done(((bf16[1408,256]{1,0:T(8,128)(2,1)}), bf16[1408,2048]{1,0:T(8,128)(2,1)}) %all-gather.12.cloned.1.call-update) | async-done | bytes 5767184 | tf_op jit(solution)/shard_map/all_gather | solution.py:59
  419.6 9.5 %convolution_convert_fusion.1 = bf16[256,2048]{1,0:T(8,128)(2,1)} fusion(bf16[1408,2048]{1,0:T(8,128)(2,1)} %all-gather.12.cloned.1.call-done, bf16[256,2048]{1,0:T(8,128)(2,1)} %all-gather.6.cloned.1.call-done, bf16[2048,1408]{1,0:T(8,128)(2,1)} %all-gather.10.cloned.1.call-done, f32[256,1408]{1,0:T(8,128)} %fusion.53), kind=kOutput, calls=%fused_computation.10 | convolution fusion | flops 2955476992 | bytes 15073280 | tf_op jit(solution)/shard_map/dot_general | solution.py:115
  429.1 0.0 reduce-scatter.5.cloned.1.call-update
  429.1 23.1 %reduce-scatter.5.cloned.1.call-done = bf16[64,2048]{1,0:T(8,128)(2,1)} async-done(((bf16[256,2048]{1,0:T(8,128)(2,1)}), bf16[64,2048]{1,0:T(8,128)(2,1)}) %reduce-scatter.5.cloned.1.call-update) | async-done | bytes 262160 | tf_op jit(solution)/shard_map/reduce_scatter | solution.py:116
  452.3 0.0 copy-done.3
  452.3 1.8 fusion.22
  (6 shorter events, 0.1 us)
Async XLA Ops:
  6.5 85.0 %copy-start = (bf16[512,2048]{1,0:T(8,128)(2,1)S(1)}, bf16[512,2048]{1,0:T(8,128)(2,1)}, u32[]{:S(2)}) copy-start(bf16[512,2048]{1,0:T(8,128)(2,1)} %param.17) | copy-start | bytes 6291460
  6.5 112.9 %reduce-scatter.3.cloned.1.call-start = ((), (), s32[]{:S(2)}) async-start(), calls=%async_computation.2 | async-start | bytes 1310720 | tf_op jit(solution)/shard_map/reduce_scatter | solution.py:100
  50.5 3.2 copy-start.1
  50.5 4.6 %copy-start.4 = (bf16[256,128]{1,0:T(8,128)(2,1)S(1)}, bf16[256,128]{1,0:T(8,128)(2,1)}, u32[]{:S(2)}) copy-start(bf16[256,128]{1,0:T(8,128)(2,1)} %param.14) | copy-start | bytes 196612
  86.5 32.9 %copy-start.2 = (bf16[64,2048]{1,0:T(8,128)(2,1)S(1)}, bf16[64,2048]{1,0:T(8,128)(2,1)}, u32[]{:S(2)}) copy-start(bf16[64,2048]{1,0:T(8,128)(2,1)} %param.11) | copy-start | bytes 786436
  86.5 34.1 %copy-start.5 = (f32[2048]{0:T(1024)S(1)}, f32[2048]{0:T(1024)}, u32[]{:S(2)}) copy-start(f32[2048]{0:T(1024)} %param.18) | copy-start | bytes 24580
  93.3 45.9 %all-gather.6.cloned.1.call-start = ((), (), s32[]{:S(2)}) async-start(), calls=%async_computation.3 | async-start | bytes 1310720 | tf_op jit(solution)/shard_map/all_gather | solution.py:111
  122.4 111.4 %all-gather.8.cloned.1.call-start = ((), (), s32[]{:S(2)}) async-start(), calls=%async_computation.4 | async-start | bytes 6488064 | tf_op jit(solution)/shard_map/all_gather | solution.py:56
  123.1 203.2 %all-gather.10.cloned.1.call-start = ((), (), s32[]{:S(2)}) async-start(), calls=%async_computation.5 | async-start | bytes 6488064 | tf_op jit(solution)/shard_map/all_gather | solution.py:57
  123.7 295.9 %all-gather.12.cloned.1.call-start = ((), (), s32[]{:S(2)}) async-start(), calls=%async_computation.6 | async-start | bytes 6488064 | tf_op jit(solution)/shard_map/all_gather | solution.py:59
  124.3 327.9 %reduce-scatter.5.cloned.1.call-start = ((), (), s32[]{:S(2)}) async-start(), calls=%async_computation.7 | async-start | bytes 1310720 | tf_op jit(solution)/shard_map/reduce_scatter | solution.py:116
  239.7 212.6 %copy-start.3 = (bf16[64,2048]{1,0:T(8,128)(2,1)S(1)}, bf16[64,2048]{1,0:T(8,128)(2,1)}, u32[]{:S(2)}) copy-start(bf16[64,2048]{1,0:T(8,128)(2,1)} %reduce-scatter.3.cloned.1.call-done) | copy-start | bytes 786436
Sparse Core Ops, SparseCore 0:
  93.4 25.9 reduce-scatter.2
  122.5 16.6 all-gather.5
  141.4 92.2 all-gather.7
  235.8 90.4 all-gather.9
  328.2 91.2 all-gather.11
  429.2 22.9 reduce-scatter.4
where the time goes:
time: 461 us
  waiting for transfers between devices  340 us (74%)
  blocking collectives  64.3 us (14%)
  matrix products  23.5 us (5%)
  other arithmetic  14.3 us (3%)
  between operations  13.6 us (3%)
    all_gather x1, waiting for transfers between devices, per_device(): lax.all_gather(gate_weight, 'sp', axis=0, tiled=True)  94.5 us
    all_gather x1, waiting for transfers between devices, per_device(): down_full = lax.all_gather(down_weight, 'sp', axis=1, tiled=True)  93.2 us
    all_gather x1, waiting for transfers between devices, per_device(): lax.all_gather(up_weight, 'sp', axis=0, tiled=True)  86.7 us
    all_gather x1, blocking collectives, per_device(): k_piece = lax.all_gather(k_rot, 'sp', axis=0, tiled=True)  33 us
    all_gather x1, blocking collectives, per_device(): v_piece = lax.all_gather(vals, 'sp', axis=0, tiled=True)  31.3 us
    reduce_scatter x1, waiting for transfers between devices, per_device(): lax.psum_scatter(jnp.dot(attended, out_weight, preferred_element_type=jnp...  26.1 us
    reduce_scatter x1, waiting for transfers between devices, per_device(): lax.psum_scatter(terms.astype(jnp.bfloat16), 'tp', scatter_dimension=0, t...  23.1 us
    all_gather x1, waiting for transfers between devices, per_device(): whole_rows = lax.all_gather(normed, 'tp', axis=0, tiled=True)  14.7 us
  transfers between devices with their start and end apart: 6, of which 6 were waited for; matrix products, arithmetic and copies ran while one was open for 1% of the time, Pallas kernels for 0%

commit v1 on v0

--- a/solution.py
+++ b/solution.py
@@ -56,7 +56,7 @@
         lax.all_gather(gate_weight, "sp", axis=0, tiled=True),
         lax.all_gather(up_weight, "sp", axis=0, tiled=True),
     )
-    down_full = lax.all_gather(down_weight, "sp", axis=1, tiled=True)
+    down_full = jnp.concatenate(lax.all_gather(down_weight, "sp"), axis=1)
     positions = lax.axis_index("sp") * tok + jnp.arange(tok, dtype=jnp.int32)
     q_rot = prepare_heads(queries, query_gain, positions, local_heads).reshape(
         tok, local_kv, group, head_dim

time: 461 us -> 436 us (0.946)
  waiting for transfers between devices: 340 us -> 304 us
  local copies, waits for them, and re-layouts: 4.56 us -> 12.9 us
    all_gather x1, waiting for transfers between devices: 93.2 us -> 65.4 us  [per_device(): down_full = jnp.concatenate(lax.all_gather(down_weight, 'sp'), axis=1)]
    reshape x0 -> x1, local copies, waits for them, and re-layouts: none -> 8.32 us  [per_device(): down_full = jnp.concatenate(lax.all_gather(down_weight, 'sp'), axis=1)]
    all_gather x1, waiting for transfers between devices: 14.7 us -> 7.86 us  [per_device(): whole_rows = lax.all_gather(normed, 'tp', axis=0, tiled=True)]
  transfers between devices with their start and end apart: 6 -> 6, of which waited for: 6 -> 6; matrix products, arithmetic and copies ran while one was open for 1% -> 4% of each run, Pallas kernels for 0% -> 0%
where the time goes in v1:
time: 436 us; the launch traced here: 435 us
  waiting for transfers between devices  304 us (70%)
  blocking collectives  64.3 us (15%)
  matrix products  23.5 us (5%)
  between operations  15.2 us (3%)
  other arithmetic  14.3 us (3%)
  local copies, waits for them, and re-layouts  12.9 us (3%)
    all_gather x1, waiting for transfers between devices, per_device(): lax.all_gather(gate_weight, 'sp', axis=0, tiled=True)  94.2 us
    all_gather x1, waiting for transfers between devices, per_device(): lax.all_gather(up_weight, 'sp', axis=0, tiled=True)  86.6 us
    all_gather x1, waiting for transfers between devices, per_device(): down_full = jnp.concatenate(lax.all_gather(down_weight, 'sp'), axis=1)  65.4 us
    all_gather x1, blocking collectives, per_device(): k_piece = lax.all_gather(k_rot, 'sp', axis=0, tiled=True)  33 us
    all_gather x1, blocking collectives, per_device(): v_piece = lax.all_gather(vals, 'sp', axis=0, tiled=True)  31.3 us
    reduce_scatter x1, waiting for transfers between devices, per_device(): lax.psum_scatter(jnp.dot(attended, out_weight, preferred_element_type=jnp...  25.5 us
    reduce_scatter x1, waiting for transfers between devices, per_device(): lax.psum_scatter(terms.astype(jnp.bfloat16), 'tp', scatter_dimension=0, t...  23.1 us
    dot_general x1, matrix products, per_device(): terms = jnp.dot(hidden, down_full, preferred_element_type=jnp.float32)  9.5 us
  transfers between devices with their start and end apart: 6, of which 6 were waited for; matrix products, arithmetic and copies ran while one was open for 4% of the time, Pallas kernels for 0%

profile of v1, /device:TPU:0, one launch (start us, length us, event | category | flops | bytes accessed | tf_op | source)
XLA Modules:
  0.0 435.1 jit_solution(1341825198377460762)
XLA Ops:
  7.4 0.0 copy-start
  7.4 0.0 reduce-scatter.3.cloned.1.call-start
  7.4 1.1 fusion.33
  8.5 0.9 fusion.35
  9.5 0.2 slice_negate_fusion.3
  9.6 0.8 broadcast_multiply_fusion.1
  10.4 1.2 fusion.39
  11.6 0.1 pad_maximum_fusion.4
  11.7 33.0 %all_gather.21 = bf16[2048,1,128]{2,0,1:T(8,128)(2,1)S(1)} all-gather(bf16[256,1,128]{2,0,1:T(8,128)(2,1)S(1)} %pad_maximum_fusion.4), channel_id=1, replica_groups=mesh['sp'=8,'tp'=4] {'sp'}, dimensions={0}, use_global_device_ids=true | all-gather | bytes 589824 | tf_op jit(solution)/shard_map/all_gather | solution.py:72
  44.8 1.1 copy.18
  45.8 0.1 multiply_reduce_fusion
  45.9 0.1 copy.19
  46.1 0.9 multiply_multiply_fusion
  46.9 0.5 slice_negate_fusion.1
  47.4 1.5 fusion.43
  48.9 0.5 fusion.41
  49.5 0.5 fusion.26
  50.0 1.3 bitcast_reduce_fusion
  51.3 0.0 copy-start.1
  51.4 0.0 copy-start.4
  51.4 3.2 copy-done.1
  54.6 1.4 fusion.1
  56.0 0.0 copy-done.4
  56.0 0.1 copy.20
  56.1 31.3 %all-gather = bf16[2048,128]{0,1:T(8,128)(2,1)S(1)} all-gather(bf16[256,128]{0,1:T(8,128)(2,1)S(1)} %copy.20), channel_id=2, replica_groups=mesh['sp'=8,'tp'=4] {'sp'}, dimensions={0}, use_global_device_ids=true | all-gather | bytes 589824 | tf_op jit(solution)/shard_map/all_gather | solution.py:73
  87.4 0.0 copy-start.2
  87.4 0.0 copy-start.5
  87.4 5.1 %fusion.16 = bf16[1,128,256,4]{2,1,3,0:T(8,128)(2,1)S(1)} fusion(f32[2048,256,4]{1,0,2:T(8,128)} %copy-done.1, f32[256,4]{0,1:T(4,128)S(1)} %get-tuple-element.50, bf16[2048,128]{0,1:T(8,128)(2,1)S(1)} %all-gather, f32[256,4]{0,1:T(4,128)S(1)} %get-tuple-element.43, f32[256,4]{0,1:T(4,128)S(1)} %get-tuple-element.42), kind=kOutput, calls=%fused_computation.14 | convolution fusion | flops 543555584 | bytes 9187328 | tf_op jit(solution)/shard_map/while/body/eval_jaxpr/qkgs,skd->qkgd/dot_general | solution.py:92
  92.5 0.0 copy-done
  92.5 1.7 convolution_convert_fusion
  94.2 0.0 reduce-scatter.3.cloned.1.call-update
  94.2 0.0 all-gather.13.cloned.1.call-start
  94.2 0.5 all-gather.13.cloned.1.call-update
  94.8 0.0 all-gather.7.cloned.1.call-start
  94.8 25.5 %reduce-scatter.3.cloned.1.call-done = bf16[64,2048]{1,0:T(8,128)(2,1)} async-done(((bf16[256,2048]{1,0:T(8,128)(2,1)}), bf16[64,2048]{1,0:T(8,128)(2,1)}) %reduce-scatter.3.cloned.1.call-update) | async-done | bytes 262160 | tf_op jit(solution)/shard_map/reduce_scatter | solution.py:100
  120.4 0.0 copy-done.2
  120.4 1.1 fusion.19
  121.5 0.0 copy-done.5
  121.5 1.8 fusion.21
  123.3 0.0 all-gather.7.cloned.1.call-update
  123.3 0.0 all-gather.9.cloned.1.call-start
  123.4 0.5 all-gather.9.cloned.1.call-update
  123.9 0.0 all-gather.11.cloned.1.call-start
  124.0 0.7 all-gather.11.cloned.1.call-update
  124.6 0.2 reduce-scatter.5.cloned.1.call-start
  124.9 65.4 %all-gather.13.cloned.1.call-done = bf16[11264,256]{1,0:T(8,128)(2,1)} async-done(((bf16[1408,256]{1,0:T(8,128)(2,1)}), bf16[11264,256]{1,0:T(8,128)(2,1)}) %all-gather.13.cloned.1.call-update) | async-done | bytes 5767184 | tf_op jit(solution)/shard_map/all_gather | solution.py:59
  190.2 8.3 %copy.22 = bf16[1408,8,256]{0,2,1:T(8,128)(2,1)} copy(bf16[1408,8,256]{2,0,1:T(8,128)(2,1)} %bitcast.75) | data formatting | bytes 11534336 | tf_op jit(solution)/shard_map/reshape | solution.py:59
  198.6 7.9 %all-gather.7.cloned.1.call-done = bf16[256,2048]{1,0:T(8,128)(2,1)} async-done(((bf16[64,2048]{1,0:T(8,128)(2,1)}), bf16[256,2048]{1,0:T(8,128)(2,1)}) %all-gather.7.cloned.1.call-update) | async-done | bytes 1048592 | tf_op jit(solution)/shard_map/all_gather | solution.py:111
  206.4 94.2 %all-gather.9.cloned.1.call-done = bf16[2048,1408]{1,0:T(8,128)(2,1)} async-done(((bf16[256,1408]{1,0:T(8,128)(2,1)}), bf16[2048,1408]{1,0:T(8,128)(2,1)}) %all-gather.9.cloned.1.call-update) | async-done | bytes 5767184 | tf_op jit(solution)/shard_map/all_gather | solution.py:56
  300.6 5.9 %fusion.53 = f32[256,1408]{1,0:T(8,128)} fusion(bf16[256,2048]{1,0:T(8,128)(2,1)} %all-gather.7.cloned.1.call-done, bf16[2048,1408]{1,0:T(8,128)(2,1)} %all-gather.9.cloned.1.call-done), kind=kOutput, calls=%fused_computation.88 | convolution fusion | flops 1476395008 | bytes 8257536 | tf_op jit(solution)/shard_map/dot_general | solution.py:112
  306.6 86.6 %all-gather.11.cloned.1.call-done = bf16[2048,1408]{1,0:T(8,128)(2,1)} async-done(((bf16[256,1408]{1,0:T(8,128)(2,1)}), bf16[2048,1408]{1,0:T(8,128)(2,1)}) %all-gather.11.cloned.1.call-update) | async-done | bytes 5767184 | tf_op jit(solution)/shard_map/all_gather | solution.py:57
  393.1 0.0 copy-start.3
  393.1 9.5 %convolution_convert_fusion.1 = bf16[256,2048]{1,0:T(8,128)(2,1)} fusion(bf16[1408,2048]{0,1:T(8,128)(2,1)} %bitcast.76, bf16[256,2048]{1,0:T(8,128)(2,1)} %all-gather.7.cloned.1.call-done, bf16[2048,1408]{1,0:T(8,128)(2,1)} %all-gather.11.cloned.1.call-done, f32[256,1408]{1,0:T(8,128)} %fusion.53), kind=kOutput, calls=%fused_computation.10 | convolution fusion | flops 2955476992 | bytes 15073280 | tf_op jit(solution)/shard_map/dot_general | solution.py:115
  402.6 0.0 reduce-scatter.5.cloned.1.call-update
  402.7 23.1 %reduce-scatter.5.cloned.1.call-done = bf16[64,2048]{1,0:T(8,128)(2,1)} async-done(((bf16[256,2048]{1,0:T(8,128)(2,1)}), bf16[64,2048]{1,0:T(8,128)(2,1)}) %reduce-scatter.5.cloned.1.call-update) | async-done | bytes 262160 | tf_op jit(solution)/shard_map/reduce_scatter | solution.py:116
  425.8 0.0 copy-done.3
  425.8 1.8 fusion.22
  (6 shorter events, 0.1 us)
Async XLA Ops:
  7.4 85.1 %copy-start = (bf16[512,2048]{1,0:T(8,128)(2,1)S(1)}, bf16[512,2048]{1,0:T(8,128)(2,1)}, u32[]{:S(2)}) copy-start(bf16[512,2048]{1,0:T(8,128)(2,1)} %param.17) | copy-start | bytes 6291460
  7.4 113.0 %reduce-scatter.3.cloned.1.call-start = ((), (), s32[]{:S(2)}) async-start(), calls=%async_computation.2 | async-start | bytes 1310720 | tf_op jit(solution)/shard_map/reduce_scatter | solution.py:100
  51.3 3.2 copy-start.1
  51.4 4.6 %copy-start.4 = (bf16[256,128]{1,0:T(8,128)(2,1)S(1)}, bf16[256,128]{1,0:T(8,128)(2,1)}, u32[]{:S(2)}) copy-start(bf16[256,128]{1,0:T(8,128)(2,1)} %param.14) | copy-start | bytes 196612
  87.4 33.0 %copy-start.2 = (bf16[64,2048]{1,0:T(8,128)(2,1)S(1)}, bf16[64,2048]{1,0:T(8,128)(2,1)}, u32[]{:S(2)}) copy-start(bf16[64,2048]{1,0:T(8,128)(2,1)} %param.11) | copy-start | bytes 786436
  87.4 34.1 %copy-start.5 = (f32[2048]{0:T(1024)S(1)}, f32[2048]{0:T(1024)}, u32[]{:S(2)}) copy-start(f32[2048]{0:T(1024)} %param.18) | copy-start | bytes 24580
  94.2 96.0 %all-gather.13.cloned.1.call-start = ((), (), s32[]{:S(2)}) async-start(), calls=%async_computation.7 | async-start | bytes 6488064 | tf_op jit(solution)/shard_map/all_gather | solution.py:59
  94.8 111.6 %all-gather.7.cloned.1.call-start = ((), (), s32[]{:S(2)}) async-start(), calls=%async_computation.3 | async-start | bytes 1310720 | tf_op jit(solution)/shard_map/all_gather | solution.py:111
  123.3 177.3 %all-gather.9.cloned.1.call-start = ((), (), s32[]{:S(2)}) async-start(), calls=%async_computation.4 | async-start | bytes 6488064 | tf_op jit(solution)/shard_map/all_gather | solution.py:56
  123.9 269.2 %all-gather.11.cloned.1.call-start = ((), (), s32[]{:S(2)}) async-start(), calls=%async_computation.5 | async-start | bytes 6488064 | tf_op jit(solution)/shard_map/all_gather | solution.py:57
  124.6 301.1 %reduce-scatter.5.cloned.1.call-start = ((), (), s32[]{:S(2)}) async-start(), calls=%async_computation.6 | async-start | bytes 1310720 | tf_op jit(solution)/shard_map/reduce_scatter | solution.py:116
  393.1 32.6 %copy-start.3 = (bf16[64,2048]{1,0:T(8,128)(2,1)S(1)}, bf16[64,2048]{1,0:T(8,128)(2,1)}, u32[]{:S(2)}) copy-start(bf16[64,2048]{1,0:T(8,128)(2,1)} %reduce-scatter.3.cloned.1.call-done) | copy-start | bytes 786436
Sparse Core Ops, SparseCore 0:
  94.3 26.0 reduce-scatter.2
  402.8 22.9 reduce-scatter.4
Sparse Core Ops, SparseCore 1:
  96.9 93.3 all-gather.12
  191.7 14.7 all-gather.6
  208.5 92.1 all-gather.8
  302.8 90.2 all-gather.10
